TPU v7x, 32 devices: a whole 2x2x4 slice. The times are simulated.
32 devices in a mesh: fs: 8 (over z, x), tp: 4 (over y, core).
Axes of the slice: x: 2, y: 2, z: 4, core: 2. Of those that a mesh axis runs over, the one named last changes fastest.
Arguments:
- tokens: bfloat16 [8192, 2048], P('fs', 'tp'), may hold values from -6 to 6
- recurrence_norm_gain: float32 [2048], replicated, may hold values from 0.1 to 1.9
- output_gate_weight: bfloat16 [2048, 2816], P('fs', 'tp'), may hold values from -0.125 to 0.125
- recurrence_input_weight: bfloat16 [2048, 2816], P('fs', 'tp'), may hold values from -0.125 to 0.125
- convolution_taps: float32 [4, 2816], P(None, 'tp'), may hold values from -3 to 3
- recurrence_gate_weight: bfloat16 [8, 352, 352], P('tp'), may hold values from -0.3125 to 0.3125
- input_gate_weight: bfloat16 [8, 352, 352], P('tp'), may hold values from -0.3125 to 0.3125
- base_decay_logit: float32 [2816], P('tp'), may hold values from 4.5 to 9.5
- token_log_decay: float32 [8192], P('fs'), may hold values from -0.7 to 0, as said below
- recurrence_output_weight: bfloat16 [2816, 2048], P('tp', 'fs'), may hold values from -0.4375 to 0.4375
- feedforward_norm_gain: float32 [2048], replicated, may hold values from 0.1 to 1.9
- feedforward_gate_weight: bfloat16 [2048, 5632], P('fs', 'tp'), may hold values from -0.125 to 0.125
- feedforward_up_weight: bfloat16 [2048, 5632], P('fs', 'tp'), may hold values from -0.125 to 0.125
- feedforward_down_weight: bfloat16 [5632, 2048], P('tp', 'fs'), may hold values from -0.15625 to 0.15625
Outputs:
- layer_out: bfloat16 [8192, 2048], P('fs', 'tp')
Inputs may be any that keep to these rules, and one draw needn't show every extreme that they name: `token_log_decay`: each entry is zero or lies between -0.7 and -0.22.
All inputs are finite; a program needn't handle non-finite values.
Results may differ from a plain program's by a relative error of at most 0.022.
Values may be sent and summed in bfloat16 or wider, within the bound.
A program may use at most 128 MiB of HBM per device.

v0:
```python
import jax
import jax.numpy as jnp
from jax import lax
from jax.sharding import PartitionSpec as P

LEN = 128


EPSILON = 1e-06
GATE_EXPONENT = 8.0


def norm_rows(values, gain_vec):
    widened = values.astype(jnp.float32)
    scaled = widened * lax.rsqrt(jnp.mean(widened * widened, axis=-1, keepdims=True) + EPSILON)
    return (scaled * gain_vec).astype(jnp.bfloat16)


def causal_taps(feature_vector, convolution_taps, length):
    row_count, channels = feature_vector.shape
    tap_count = convolution_taps.shape[0]
    blocks = feature_vector.reshape(row_count // length, length, channels)
    target = lax.broadcasted_iota(jnp.int32, (tap_count, length, length), 1)
    source = lax.broadcasted_iota(jnp.int32, (tap_count, length, length), 2)
    offset = lax.broadcasted_iota(jnp.int32, (tap_count, length, length), 0)
    shifters = (source == target - (tap_count - 1) + offset).astype(jnp.bfloat16)
    shifted = jnp.einsum("kts,bsc->kbtc", shifters, blocks, preferred_element_type=jnp.float32)
    summed = convolution_taps[0] * shifted[0]
    for position in range(1, tap_count):
        summed = summed + convolution_taps[position] * shifted[position]
    return summed.reshape(row_count, channels).astype(jnp.bfloat16)


def combine_steps(earlier, latter):
    return (earlier[0] * latter[0], latter[0] * earlier[1] + latter[1])


def linear_scan(decays, driven, length):
    row_count, channels = decays.shape
    shaped = (
        decays.reshape(row_count // length, length, channels),
        driven.reshape(row_count // length, length, channels),
    )
    result = lax.associative_scan(combine_steps, shaped, axis=1)
    return result[1].reshape(row_count, channels)


def block_dense(weight):
    groups, block_width, _ = weight.shape
    identity = jnp.eye(groups, dtype=jnp.bfloat16)[:, None, :, None]
    return (weight[:, :, None, :] * identity).reshape(groups * block_width, groups * block_width)


def two_projections(normed, collected):
    return (
        jnp.dot(normed, collected[0], preferred_element_type=jnp.float32),
        jnp.dot(normed, collected[1], preferred_element_type=jnp.float32),
    )


def project_down(values, weight):
    return jnp.dot(
        values, lax.all_gather(weight, "fs", axis=1, tiled=True), preferred_element_type=jnp.float32
    )


def recurrence(
    gate_projected,
    feature_vector,
    convolution_taps,
    recurrence_gate_weight,
    input_gate_weight,
    base_decay_logit,
    token_log_decay,
):
    mixed_in = causal_taps(feature_vector, convolution_taps, LEN)
    recurrence_gate = jax.nn.sigmoid(
        jnp.dot(mixed_in, block_dense(recurrence_gate_weight), preferred_element_type=jnp.float32)
    )
    inject_gate = jax.nn.sigmoid(
        jnp.dot(mixed_in, block_dense(input_gate_weight), preferred_element_type=jnp.float32)
    )
    decay_log_value = (
        -GATE_EXPONENT * jax.nn.softplus(-base_decay_logit)[None, :] * recurrence_gate
        + token_log_decay[:, None]
    )
    decays = jnp.exp(decay_log_value)
    driven = jnp.sqrt(-jnp.expm1(2.0 * decay_log_value)) * (
        inject_gate * mixed_in.astype(jnp.float32)
    )
    states = linear_scan(decays, driven, LEN)
    return (states * jax.nn.gelu(gate_projected)).astype(jnp.bfloat16)


def shards(
    tokens,
    recurrence_norm_gain,
    output_gate_weight,
    recurrence_input_weight,
    convolution_taps,
    recurrence_gate_weight,
    input_gate_weight,
    base_decay_logit,
    token_log_decay,
    recurrence_output_weight,
    feedforward_norm_gain,
    feedforward_gate_weight,
    feedforward_up_weight,
    feedforward_down_weight,
):
    collected = (
        lax.all_gather(output_gate_weight, "fs", axis=0, tiled=True),
        lax.all_gather(recurrence_input_weight, "fs", axis=0, tiled=True),
        lax.all_gather(feedforward_gate_weight, "fs", axis=0, tiled=True),
        lax.all_gather(feedforward_up_weight, "fs", axis=0, tiled=True),
    )
    full_rows = lax.all_gather(tokens, "tp", axis=1, tiled=True)
    normed = norm_rows(full_rows, recurrence_norm_gain)
    gate_projected, feature_vector = two_projections(normed, collected[0:2])
    carried = recurrence(
        gate_projected,
        feature_vector.astype(jnp.bfloat16),
        convolution_taps,
        recurrence_gate_weight,
        input_gate_weight,
        base_decay_logit,
        token_log_decay,
    )
    mixer_term = project_down(carried, recurrence_output_weight)
    own_sum = lax.psum_scatter(
        mixer_term.astype(jnp.bfloat16), "tp", scatter_dimension=1, tiled=True
    ).astype(jnp.float32)
    residual_own = (tokens.astype(jnp.float32) + own_sum).astype(jnp.bfloat16)
    residual_full = lax.all_gather(residual_own, "tp", axis=1, tiled=True)
    normed_two = norm_rows(residual_full, feedforward_norm_gain)
    gate_hidden, up_hidden = two_projections(normed_two, collected[2:4])
    hidden = (jax.nn.silu(gate_hidden) * up_hidden).astype(jnp.bfloat16)
    down_term = project_down(hidden, feedforward_down_weight)
    own_down = lax.psum_scatter(
        down_term.astype(jnp.bfloat16), "tp", scatter_dimension=1, tiled=True
    ).astype(jnp.float32)
    return (residual_own.astype(jnp.float32) + own_down).astype(jnp.bfloat16)


def solution(mesh):
    in_specs = (
        P("fs", "tp"),
        P(),
        P("fs", "tp"),
        P("fs", "tp"),
        P(None, "tp"),
        P("tp", None, None),
        P("tp", None, None),
        P("tp"),
        P("fs"),
        P("tp", "fs"),
        P(),
        P("fs", "tp"),
        P("fs", "tp"),
        P("tp", "fs"),
    )
    out_specs = P("fs", "tp")
    return jax.shard_map(shards, mesh=mesh, in_specs=in_specs, out_specs=out_specs, check_vma=False)
```

profile of v0, /device:TPU:0, one launch (start us, length us, event | category | flops | bytes accessed | tf_op | source)
XLA Modules:
  0.0 1082.4 jit_solution(1734964078290439983)
XLA Ops:
  10.3 3.4 broadcast_multiply_fusion
  15.5 30.6 %all-gather.9.cloned.1.call-done = bf16[1024,2048]{1,0:T(8,128)(2,1)} async-done(((bf16[1024,512]{1,0:T(8,128)(2,1)}), bf16[1024,2048]{1,0:T(8,128)(2,1)}) %all-gather.9.cloned.1.call-update) | async-done | bytes 4194320 | tf_op jit(solution)/shard_map/all_gather | solution.py:117
  46.1 3.1 fusion
  49.2 58.5 %all-gather.11.cloned.1.call-done = bf16[2048,704]{0,1:T(8,128)(2,1)} async-done(((bf16[256,704]{0,1:T(8,128)(2,1)}), bf16[2048,704]{0,1:T(8,128)(2,1)}) %all-gather.11.cloned.1.call-update) | async-done | bytes 2883600 | tf_op jit(solution)/shard_map/all_gather | solution.py:113
  107.7 6.3 fusion.20
  114.5 1.8 convolution_bitcast_fusion
  116.3 2.9 fusion.57
  119.2 0.9 copy.46
  120.1 1.7 copy.47
  121.8 1.7 copy.48
  123.5 1.7 copy.49
  125.2 1.7 copy.50
  126.9 1.8 multiply_add_fusion
  128.6 5.0 multiply_bitcast_fusion
  134.3 51.8 %slice.194 = f32[8,64,704]{1,0,2:T(8,128)} slice(f32[8,128,704]{1,0,2:T(8,128)S(1)} %bitcast.97), slice={[0:8:1], [0:127:2], [0:704:1]} | slice | bytes 2883584 | tf_op jit(solution)/shard_map/slice | solution.py:44
  186.1 56.3 %slice.195 = f32[8,64,704]{1,0,2:T(8,128)} slice(f32[8,128,704]{1,0,2:T(8,128)S(1)} %bitcast.98), slice={[0:8:1], [1:128:2], [0:704:1]} | slice | bytes 2883584 | tf_op jit(solution)/shard_map/slice | solution.py:44
  242.4 2.2 exponential_bitcast_fusion
  244.6 2.4 copy.76
  246.9 52.7 %slice.193 = f32[8,64,704]{1,0,2:T(8,128)} slice(f32[8,128,704]{1,0,2:T(8,128)} %bitcast.101), slice={[0:8:1], [1:128:2], [0:704:1]} | slice | bytes 2883584 | tf_op jit(solution)/shard_map/slice | solution.py:44
  299.6 51.8 %slice.197 = f32[8,64,704]{1,0,2:T(8,128)} slice(f32[8,128,704]{1,0,2:T(8,128)} %bitcast.102), slice={[0:8:1], [0:127:2], [0:704:1]} | slice | bytes 2883584 | tf_op jit(solution)/shard_map/slice | solution.py:44
  351.5 55.5 %slice.241 = f32[8,63,704]{1,0,2:T(8,128)} slice(f32[8,128,704]{1,0,2:T(8,128)S(1)} %bitcast.99), slice={[0:8:1], [2:128:2], [0:704:1]} | slice | bytes 2838528 | tf_op jit(solution)/shard_map/slice | solution.py:44
  407.0 52.1 %slice.192 = f32[8,63,704]{1,0,2:T(8,128)} slice(f32[8,128,704]{1,0,2:T(8,128)} %bitcast.103), slice={[0:8:1], [2:128:2], [0:704:1]} | slice | bytes 2838528 | tf_op jit(solution)/shard_map/slice | solution.py:44
  459.1 3.3 copy.65
  462.3 3.3 copy.66
  465.6 3.3 copy.64
  468.9 3.3 copy.67
  472.1 3.2 fusion.58
  480.7 1.5 pad.48
  482.2 1.0 fusion.47
  483.2 1.4 pad_maximum_fusion.4
  484.6 3.4 pad.47
  488.0 1.6 add.195
  489.6 1.0 fusion.45
  490.8 5.0 pad.50
  495.7 1.8 add.197
  497.5 8.9 pad.52
  506.5 1.3 fusion.42
  507.8 5.8 pad.51
  513.5 2.4 add.199
  515.9 2.0 fusion.41
  518.8 16.1 %pad.53 = f32[8,64,704]{2,0,1:T(8,128)} pad(f32[8,32,704]{2,0,1:T(8,128)} %pad_maximum_fusion.1, f32[]{:T(128)} %constant.10.clone.1), padding=0_0_0x0_1_1x0_0_0 | pad | bytes 2162692 | tf_op jit(solution)/shard_map/pad | solution.py:44
  535.0 16.1 %pad.54 = f32[8,64,704]{2,0,1:T(8,128)} pad(f32[8,32,704]{2,0,1:T(8,128)} %add.199, f32[]{:T(128)} %constant.10.clone.1), padding=0_0_0x1_0_1x0_0_0 | pad | bytes 2162692 | tf_op jit(solution)/shard_map/pad | solution.py:44
  551.0 3.2 add.201
  554.3 31.2 %pad.56 = f32[8,128,704]{2,0,1:T(8,128)} pad(f32[8,64,704]{2,0,1:T(8,128)} %add.201, f32[]{:T(128)} %constant.10.clone.1), padding=0_0_0x1_0_1x0_0_0 | pad | bytes 4325380 | tf_op jit(solution)/shard_map/pad | solution.py:44
  585.5 3.3 copy.68
  588.8 3.4 copy.63
  592.2 1.0 copy.62
  593.3 3.2 fusion.19
  596.5 1.3 pad_maximum_fusion
  597.7 31.5 %pad.55 = f32[8,128,704]{2,0,1:T(8,128)} pad(f32[8,64,704]{2,0,1:T(8,128)} %pad_maximum_fusion, f32[]{:T(128)} %constant.10.clone.1), padding=0_0_0x0_1_1x0_0_0 | pad | bytes 4325380 | tf_op jit(solution)/shard_map/pad | solution.py:44
  629.3 4.0 add.203
  633.3 2.6 copy.58
  636.0 12.7 %convolution_convert_fusion.1 = bf16[1024,2048]{1,0:T(8,128)(2,1)} fusion(bf16[704,2048]{1,0:T(8,128)(2,1)} %all-gather.15.cloned.1.call-done, f32[88,8,8,128]{3,2,1,0:T(8,128)S(1)} %bitcast.109, bf16[2048,704]{0,1:T(8,128)(2,1)} %all-gather.13.cloned.1.call-done, bf16[1024,2048]{1,0:T(8,128)(2,1)} %all-gather.9.cloned.1.call-done, ...), kind=kOutput, calls=%fused_computation.14 | convolution fusion | flops 5923274752 | bytes 17051648 | tf_op jit(solution)/shard_map/dot_general | solution.py:62
  648.8 42.7 %reduce-scatter.3.cloned.1.call-done = bf16[1024,512]{1,0:T(8,128)(2,1)} async-done(((bf16[1024,2048]{1,0:T(8,128)(2,1)}), bf16[1024,512]{1,0:T(8,128)(2,1)}) %reduce-scatter.3.cloned.1.call-update) | async-done | bytes 1048592 | tf_op jit(solution)/shard_map/reduce_scatter | solution.py:130
  691.5 2.5 add_convert_fusion.2
  696.3 32.3 %all-gather.17.cloned.1.call-done = bf16[1024,2048]{1,0:T(8,128)(2,1)} async-done(((bf16[1024,512]{1,0:T(8,128)(2,1)}), bf16[1024,2048]{1,0:T(8,128)(2,1)}) %all-gather.17.cloned.1.call-update) | async-done | bytes 4194320 | tf_op jit(solution)/shard_map/all_gather | solution.py:134
  728.6 3.1 fusion.3
  731.7 91.4 %all-gather.19.cloned.1.call-done = bf16[2048,1408]{1,0:T(8,128)(2,1)} async-done(((bf16[256,1408]{1,0:T(8,128)(2,1)}), bf16[2048,1408]{1,0:T(8,128)(2,1)}) %all-gather.19.cloned.1.call-update) | async-done | bytes 5767184 | tf_op jit(solution)/shard_map/all_gather | solution.py:114
  823.1 12.1 %fusion.32 = f32[1024,1408]{1,0:T(8,128)} fusion(bf16[2048,1408]{1,0:T(8,128)(2,1)} %all-gather.19.cloned.1.call-done, bf16[1024,2048]{1,0:T(8,128)(2,1)} %all-gather.17.cloned.1.call-done, f32[2048]{0:T(1024)S(1)} %copy-done.18, f32[1024]{0:T(1024)S(1)} %add_rsqrt_fusion), kind=kOutput, calls=%fused_computation.53 | convolution fusion | flops 5913968640 | bytes 15740928 | tf_op jit(solution)/shard_map/dot_general | solution.py:56
  835.2 80.6 %all-gather.21.cloned.1.call-done = bf16[2048,1408]{1,0:T(8,128)(2,1)} async-done(((bf16[256,1408]{1,0:T(8,128)(2,1)}), bf16[2048,1408]{1,0:T(8,128)(2,1)}) %all-gather.21.cloned.1.call-update) | async-done | bytes 5767184 | tf_op jit(solution)/shard_map/all_gather | solution.py:115
  915.8 93.4 %all-gather.23.cloned.1.call-done = bf16[1408,2048]{1,0:T(8,128)(2,1)} async-done(((bf16[1408,256]{1,0:T(8,128)(2,1)}), bf16[1408,2048]{1,0:T(8,128)(2,1)}) %all-gather.23.cloned.1.call-update) | async-done | bytes 5767184 | tf_op jit(solution)/shard_map/all_gather | solution.py:63
  1009.2 20.9 %convolution_convert_fusion = bf16[1024,2048]{1,0:T(8,128)(2,1)} fusion(bf16[1408,2048]{1,0:T(8,128)(2,1)} %all-gather.23.cloned.1.call-done, f32[1024,1408]{1,0:T(8,128)} %fusion.32, bf16[2048,1408]{1,0:T(8,128)(2,1)} %all-gather.21.cloned.1.call-done, bf16[1024,2048]{1,0:T(8,128)(2,1)} %all-gather.17.cloned.1.call-done, f32[2048]{0:T(1024)S(1)} %copy-done.18, ...), kind=kOutput, calls=%fused_computation.13 | convolution fusion | flops 11830296576 | bytes 25702400 | tf_op jit(solution)/shard_map/dot_general | solution.py:62
  1030.1 42.7 %reduce-scatter.5.cloned.1.call-done = bf16[1024,512]{1,0:T(8,128)(2,1)} async-done(((bf16[1024,2048]{1,0:T(8,128)(2,1)}), bf16[1024,512]{1,0:T(8,128)(2,1)}) %reduce-scatter.5.cloned.1.call-update) | async-done | bytes 1048592 | tf_op jit(solution)/shard_map/reduce_scatter | solution.py:139
  1072.9 2.5 add_convert_fusion.1
  (92 shorter events, 15.2 us)
Async XLA Ops:
  6.5 39.6 %all-gather.9.cloned.1.call-start = ((), (), s32[]{:S(2)}) async-start(), calls=%async_computation.2 | async-start | bytes 5242880 | tf_op jit(solution)/shard_map/all_gather | solution.py:117
  7.3 100.5 %all-gather.11.cloned.1.call-start = ((), (), s32[]{:S(2)}) async-start(), calls=%async_computation.3 | async-start | bytes 3244032 | tf_op jit(solution)/shard_map/all_gather | solution.py:113
  8.0 628.0 %all-gather.13.cloned.1.call-start = ((), (), s32[]{:S(2)}) async-start(), calls=%async_computation.4 | async-start | bytes 3244032 | tf_op jit(solution)/shard_map/all_gather | solution.py:112
  8.7 5.8 copy-start.15
  8.8 627.2 %all-gather.15.cloned.1.call-start = ((), (), s32[]{:S(2)}) async-start(), calls=%async_computation.5 | async-start | bytes 3244032 | tf_op jit(solution)/shard_map/all_gather | solution.py:63
  9.3 682.2 %reduce-scatter.3.cloned.1.call-start = ((), (), s32[]{:S(2)}) async-start(), calls=%async_computation.6 | async-start | bytes 5242880 | tf_op jit(solution)/shard_map/reduce_scatter | solution.py:130
  14.6 93.2 %copy-start.16 = (f32[2048]{0:T(1024)S(1)}, f32[2048]{0:T(1024)}, u32[]{:S(2)}) copy-start(f32[2048]{0:T(1024)} %param.15) | copy-start | bytes 24580
  125.2 1.7 copy-start.19
  128.6 5.0 copy-start.7
  475.4 1.1 copy-start.1
  475.4 1.7 copy-start.2
  476.2 1.0 copy-start.4
  476.3 1.6 copy-start.5
  477.0 0.8 copy-start.8
  477.9 0.7 copy-start.9
  477.9 0.7 copy-start.10
  478.8 0.6 copy-start.11
  479.4 0.6 copy-start.12
  480.1 10.6 copy-start.13
  513.5 4.4 copy-start.14
  597.7 31.5 %copy-start = (f32[8,128,704]{2,0,1:T(8,128)S(1)}, f32[8,128,704]{2,0,1:T(8,128)}, u32[]{:S(2)}) copy-start(f32[8,128,704]{2,0,1:T(8,128)} %pad.56) | copy-start | bytes 8650756
  633.3 2.7 copy-start.17
  648.7 42.8 %copy-start.6 = (bf16[1024,512]{1,0:T(8,128)(2,1)S(1)}, bf16[1024,512]{1,0:T(8,128)(2,1)}, u32[]{:S(2)}) copy-start(bf16[1024,512]{1,0:T(8,128)(2,1)} %param.14) | copy-start | bytes 3145732
  648.7 79.9 %all-gather.17.cloned.1.call-start = ((), (), s32[]{:S(2)}) async-start(), calls=%async_computation.7 | async-start | bytes 5242880 | tf_op jit(solution)/shard_map/all_gather | solution.py:134
  694.0 129.1 %all-gather.19.cloned.1.call-start = ((), (), s32[]{:S(2)}) async-start(), calls=%async_computation.8 | async-start | bytes 6488064 | tf_op jit(solution)/shard_map/all_gather | solution.py:114
  694.7 128.4 %copy-start.18 = (f32[2048]{0:T(1024)S(1)}, f32[2048]{0:T(1024)}, u32[]{:S(2)}) copy-start(f32[2048]{0:T(1024)} %param.24) | copy-start | bytes 24580
  694.8 221.1 %all-gather.21.cloned.1.call-start = ((), (), s32[]{:S(2)}) async-start(), calls=%async_computation.9 | async-start | bytes 6488064 | tf_op jit(solution)/shard_map/all_gather | solution.py:115
  695.5 313.7 %all-gather.23.cloned.1.call-start = ((), (), s32[]{:S(2)}) async-start(), calls=%async_computation.10 | async-start | bytes 6488064 | tf_op jit(solution)/shard_map/all_gather | solution.py:63
  696.2 376.6 %reduce-scatter.5.cloned.1.call-start = ((), (), s32[]{:S(2)}) async-start(), calls=%async_computation.11 | async-start | bytes 5242880 | tf_op jit(solution)/shard_map/reduce_scatter | solution.py:139
  1030.1 42.8 %copy-start.3 = (bf16[1024,512]{1,0:T(8,128)(2,1)S(1)}, bf16[1024,512]{1,0:T(8,128)(2,1)}, u32[]{:S(2)}) copy-start(bf16[1024,512]{1,0:T(8,128)(2,1)} %add_convert_fusion.2) | copy-start | bytes 3145732
Sparse Core Ops, SparseCore 0:
  8.9 37.1 all-gather.8
  48.1 59.5 all-gather.10
  109.8 57.8 all-gather.12
  169.6 57.7 all-gather.14
  648.9 42.5 reduce-scatter.2
  694.1 34.4 all-gather.16
  730.8 92.2 all-gather.18
  825.3 90.4 all-gather.20
  917.9 91.2 all-gather.22
  1030.3 42.5 reduce-scatter.4
where the time goes:
time: 1100 us; the launch traced here: 1080 us
  local copies, waits for them, and re-layouts  483 us (44%)
  waiting for transfers between devices  477 us (43%)
  matrix products  60.6 us (6%)
  other arithmetic  46.9 us (4%)
  between operations  14.2 us (1%)
    slice x10, local copies, waits for them, and re-layouts, linear_scan(): result = lax.associative_scan(combine_steps, shaped, axis=1)  322 us
    pad x12, local copies, waits for them, and re-layouts, linear_scan(): result = lax.associative_scan(combine_steps, shaped, axis=1)  120 us
    all_gather x2, waiting for transfers between devices, project_down(): lax.all_gather(weight, 'fs', axis=1, tiled=True)  93.4 us
    all_gather x1, waiting for transfers between devices, shards(): lax.all_gather(feedforward_gate_weight, 'fs', axis=0, tiled=True)  91.4 us
    all_gather x1, waiting for transfers between devices, shards(): lax.all_gather(feedforward_up_weight, 'fs', axis=0, tiled=True)  80.6 us
    all_gather x1, waiting for transfers between devices, shards(): lax.all_gather(recurrence_input_weight, 'fs', axis=0, tiled=True)  58.5 us
    reduce_scatter x1, waiting for transfers between devices, shards(): lax.psum_scatter(down_term.astype(jnp.bfloat16), 'tp', scatter_dimension=...  42.7 us
    reduce_scatter x1, waiting for transfers between devices, shards(): lax.psum_scatter(mixer_term.astype(jnp.bfloat16), 'tp', scatter_dimension...  42.7 us
  transfers between devices with their start and end apart: 10, of which 8 were waited for; matrix products, arithmetic and copies ran while one was open for 51% of the time, Pallas kernels for 0%

commit v1 on v0

v1 whole, which is shorter than its diff:
```python
import functools

import jax
import jax.numpy as jnp
from jax import lax
from jax.experimental import pallas as pl
from jax.experimental.pallas import tpu as pltpu
from jax.sharding import PartitionSpec as P


LEN = 128
EPSILON = 1e-06
GATE_EXPONENT = 8.0


def ring_order(count):
    return tuple(range(0, count, 2)) + tuple(range(count - 1, 0, -2))


def ring_tables(count):
    order = ring_order(count)
    place = [0] * count
    for spot, index in enumerate(order):
        place[index] = spot
    shifts = [0]
    for step in range(1, count // 2):
        shifts += [-step, step]
    shifts.append(count // 2)
    table = [[order[(place[index] + shift) % count] for shift in shifts] for index in range(count)]
    return jnp.array(table, jnp.int32)[lax.axis_index("fs")]


def ring_gather(piece, count):
    order = ring_order(count)
    right = [(order[i], order[(i + 1) % count]) for i in range(count)]
    left = [(order[i], order[(i - 1) % count]) for i in range(count)]

    def hop(value, pairs):
        return lax.ppermute(value, "fs", pairs)

    found = [piece]
    forward = backward = piece
    half = count // 2
    for _ in range(1, half):
        forward = hop(forward, right)
        backward = hop(backward, left)
        found += [forward, backward]
    cut = piece.shape[0] // 2
    found.append(hop(forward[:cut], right))
    found.append(hop(backward[cut:], left))
    return found


def collect(owners_ref, pieces, whole_ref):
    rows = pieces[0].shape[1]
    for k, piece in enumerate(pieces[:-2]):
        spot = pl.ds(pl.multiple_of(owners_ref[k] * rows, rows), rows)
        for lead in range(2):
            whole_ref[lead, spot, :] = piece[lead]
    spot = pl.ds(pl.multiple_of(owners_ref[len(pieces) - 2] * rows, rows), rows)
    for lead in range(2):
        whole_ref[lead, spot, :] = pieces[len(pieces) - 2 + lead][0]


def norm_block(values_ref, gain_ref):
    widened = values_ref[...].astype(jnp.float32)
    scaled = widened * lax.rsqrt(jnp.mean(widened * widened, axis=-1, keepdims=True) + EPSILON)
    return (scaled * gain_ref[...]).astype(jnp.bfloat16)


ROWS = 2 * LEN
ORDERED = pltpu.CompilerParams(dimension_semantics=("arbitrary",), vmem_limit_bytes=60 * 1024 * 1024)


def once(shape):
    zeros = (0,) * len(shape)
    return pl.BlockSpec(shape, lambda i, *_: zeros, pipeline_mode=pl.Buffered(1))


def block_dense(weight):
    groups, block_width, _ = weight.shape
    identity = jnp.eye(groups, dtype=jnp.bfloat16)[:, None, :, None]
    return (weight[:, :, None, :] * identity).reshape(groups * block_width, groups * block_width)


def shift_down(values, amount, place, fill):
    return jnp.where(place >= amount, pltpu.roll(values, amount, 0), fill)


def mixer_kernel(owners_ref, rows_ref, gain_ref, taps_ref, recur_ref, inject_ref, rate_ref, token_ref, *rest):
    pieces, (out_ref, whole_ref) = rest[:-2], rest[-2:]

    @pl.when(pl.program_id(0) == 0)
    def _():
        collect(owners_ref, pieces, whole_ref)

    normed = norm_block(rows_ref, gain_ref)
    feature = jnp.dot(normed, whole_ref[1], preferred_element_type=jnp.float32)
    feature = feature.astype(jnp.bfloat16).astype(jnp.float32)
    place = lax.rem(lax.broadcasted_iota(jnp.int32, feature.shape, 0), LEN)
    taps = taps_ref[...]
    tap_count = taps.shape[0]
    summed = None
    for k in range(tap_count):
        amount = tap_count - 1 - k
        moved = shift_down(feature, amount, place, 0.0) if amount else feature
        term = taps[k : k + 1] * moved
        summed = term if summed is None else summed + term
    mixed = summed.astype(jnp.bfloat16)
    recur = jax.nn.sigmoid(jnp.dot(mixed, recur_ref[...], preferred_element_type=jnp.float32))
    inject = jax.nn.sigmoid(jnp.dot(mixed, inject_ref[...], preferred_element_type=jnp.float32))
    log_decay = rate_ref[...] * recur + token_ref[...]
    decay = jnp.exp(log_decay)
    y = 2.0 * log_decay
    series = -y * (
        1.0 + y * (1 / 2) * (1.0 + y * (1 / 3) * (1.0 + y * (1 / 4) * (1.0 + y * (1 / 5) * (1.0 + y * (1 / 6)))))
    )
    loss = jnp.where(y > -0.25, series, 1.0 - decay * decay)
    state = jnp.sqrt(loss) * (inject * mixed.astype(jnp.float32))
    amount = 1
    while amount < LEN:
        state = state + decay * shift_down(state, amount, place, 0.0)
        if 2 * amount < LEN:
            decay = decay * shift_down(decay, amount, place, 1.0)
        amount *= 2
    gate = jnp.dot(normed, whole_ref[0], preferred_element_type=jnp.float32)
    out_ref[...] = (state * jax.nn.gelu(gate)).astype(jnp.bfloat16)


def mixer(owners, full_rows, gain, taps, recur_weight, inject_weight, base_decay_logit, token_log_decay, pieces):
    rows, width = full_rows.shape
    channels = pieces[0].shape[-1]
    rate = -GATE_EXPONENT * jax.nn.softplus(-base_decay_logit)[None, :]
    block = lambda cols: pl.BlockSpec((ROWS, cols), lambda i, *_: (i, 0))
    return pl.pallas_call(
        mixer_kernel,
        grid_spec=pltpu.PrefetchScalarGridSpec(
            num_scalar_prefetch=1,
            grid=(rows // ROWS,),
            in_specs=[
                block(width),
                once((1, width)),
                once(taps.shape),
                once((channels, channels)),
                once((channels, channels)),
                once((1, channels)),
                block(1),
            ]
            + [once(piece.shape) for piece in pieces],
            out_specs=block(channels),
            scratch_shapes=[pltpu.VMEM((2, width, channels), jnp.bfloat16)],
        ),
        out_shape=jax.ShapeDtypeStruct((rows, channels), jnp.bfloat16),
        compiler_params=ORDERED,
        cost_estimate=pl.CostEstimate(
            flops=4 * rows * channels * (channels + width), bytes_accessed=4 * width * channels, transcendentals=0
        ),
    )(
        owners,
        full_rows,
        gain[None],
        taps,
        block_dense(recur_weight),
        block_dense(inject_weight),
        rate,
        token_log_decay[:, None],
        *pieces,
    )


def hidden_kernel(owners_ref, rows_ref, gain_ref, *rest):
    pieces, (out_ref, whole_ref) = rest[:-2], rest[-2:]

    @pl.when(pl.program_id(0) == 0)
    def _():
        collect(owners_ref, pieces, whole_ref)

    normed = norm_block(rows_ref, gain_ref)
    gate = jnp.dot(normed, whole_ref[0], preferred_element_type=jnp.float32)
    up = jnp.dot(normed, whole_ref[1], preferred_element_type=jnp.float32)
    out_ref[...] = (jax.nn.silu(gate) * up).astype(jnp.bfloat16)


def hidden_units(owners, full_rows, gain, pieces):
    rows, width = full_rows.shape
    units = pieces[0].shape[-1]
    block = lambda cols: pl.BlockSpec((ROWS, cols), lambda i, *_: (i, 0))
    return pl.pallas_call(
        hidden_kernel,
        grid_spec=pltpu.PrefetchScalarGridSpec(
            num_scalar_prefetch=1,
            grid=(rows // ROWS,),
            in_specs=[block(width), once((1, width))] + [once(piece.shape) for piece in pieces],
            out_specs=block(units),
            scratch_shapes=[pltpu.VMEM((2, width, units), jnp.bfloat16)],
        ),
        out_shape=jax.ShapeDtypeStruct((rows, units), jnp.bfloat16),
        compiler_params=ORDERED,
        cost_estimate=pl.CostEstimate(
            flops=4 * rows * units * width, bytes_accessed=4 * width * units, transcendentals=0
        ),
    )(owners, full_rows, gain[None], *pieces)


def down_kernel(groups, where_ref, values_ref, *rest):
    pieces, (mine_ref, other_ref) = rest[:-2], rest[-2:]
    values = values_ref[...]
    cols = pieces[0].shape[1]
    width = mine_ref.shape[2]
    y, core = where_ref[len(pieces)], where_ref[len(pieces) + 1]
    for k, piece in enumerate(pieces):
        term = jnp.dot(values, piece[...], preferred_element_type=jnp.float32).astype(jnp.bfloat16)
        start = where_ref[k] * cols
        target = start // width
        offset = pl.multiple_of(lax.rem(start, width), cols)
        turn = lax.rem(target // 2 - y + groups, groups)
        same = lax.rem(target, 2) == core

        @pl.when(same)
        def _():
            mine_ref[turn, :, pl.ds(offset, cols)] = term

        @pl.when(jnp.logical_not(same))
        def _():
            other_ref[turn, :, pl.ds(offset, cols)] = term


def project_down(owners, values, pieces, tp):
    rows, depth = values.shape
    cols = pieces[0].shape[1]
    width = cols * len(pieces) // tp
    groups = tp // 2
    tall = min(rows, 2 * ROWS)
    index = lax.axis_index("tp")
    where = jnp.concatenate([owners, jnp.stack([index // 2, index % 2]).astype(jnp.int32)])
    out_spec = pl.BlockSpec((groups, tall, width), lambda i, *_: (0, i, 0))
    shape = jax.ShapeDtypeStruct((groups, rows, width), jnp.bfloat16)
    return pl.pallas_call(
        functools.partial(down_kernel, groups),
        grid_spec=pltpu.PrefetchScalarGridSpec(
            num_scalar_prefetch=1,
            grid=(rows // tall,),
            in_specs=[pl.BlockSpec((tall, depth), lambda i, *_: (i, 0))] + [once(piece.shape) for piece in pieces],
            out_specs=[out_spec, out_spec],
        ),
        out_shape=[shape, shape],
        compiler_params=ORDERED,
        cost_estimate=pl.CostEstimate(
            flops=2 * rows * depth * cols * len(pieces), bytes_accessed=2 * depth * cols * len(pieces), transcendentals=0
        ),
    )(where, values, *pieces)


def scatter_sum(mine, other, tp):
    groups = tp // 2
    got = lax.ppermute(other, "tp", [(i, i ^ 1) for i in range(tp)])
    widen = lambda value: value.astype(jnp.float32)
    total = None
    for turn in range(1, groups):
        pair = (widen(mine[turn]) + widen(got[turn])).astype(jnp.bfloat16)
        perm = [(i, (i + 2 * turn) % tp) for i in range(tp)]
        arrived = widen(lax.ppermute(pair, "tp", perm))
        total = arrived if total is None else total + arrived
    own = widen(mine[0]) + widen(got[0])
    return own if total is None else own + total


def join_last(pieces):
    return pieces[:-2] + [jnp.concatenate(pieces[-2:], axis=0)]


def shards(
    count,
    tp,
    tokens,
    recurrence_norm_gain,
    output_gate_weight,
    recurrence_input_weight,
    convolution_taps,
    recurrence_gate_weight,
    input_gate_weight,
    base_decay_logit,
    token_log_decay,
    recurrence_output_weight,
    feedforward_norm_gain,
    feedforward_gate_weight,
    feedforward_up_weight,
    feedforward_down_weight,
):
    owners = ring_tables(count)
    first = ring_gather(jnp.stack([output_gate_weight, recurrence_input_weight]), count)
    out_pieces = join_last(ring_gather(recurrence_output_weight, count))
    second = ring_gather(jnp.stack([feedforward_gate_weight, feedforward_up_weight]), count)
    down_pieces = join_last(ring_gather(feedforward_down_weight, count))

    full_rows = lax.all_gather(tokens, "tp", axis=1, tiled=True)
    carried = mixer(
        owners,
        full_rows,
        recurrence_norm_gain,
        convolution_taps,
        recurrence_gate_weight,
        input_gate_weight,
        base_decay_logit,
        token_log_decay,
        first,
    )
    mine, other = project_down(owners, carried, out_pieces, tp)
    own_sum = scatter_sum(mine, other, tp)
    residual_own = (tokens.astype(jnp.float32) + own_sum).astype(jnp.bfloat16)
    residual_full = lax.all_gather(residual_own, "tp", axis=1, tiled=True)
    hidden = hidden_units(owners, residual_full, feedforward_norm_gain, second)
    chunks = 2 if hidden.shape[0] % (2 * ROWS) == 0 else 1
    size = hidden.shape[0] // chunks
    sums = []
    for chunk in range(chunks):
        mine, other = project_down(owners, hidden[chunk * size : (chunk + 1) * size], down_pieces, tp)
        sums.append(scatter_sum(mine, other, tp))
    own_down = jnp.concatenate(sums, axis=0)
    return (residual_own.astype(jnp.float32) + own_down).astype(jnp.bfloat16)


def solution(mesh):
    in_specs = (
        P("fs", "tp"),
        P(),
        P("fs", "tp"),
        P("fs", "tp"),
        P(None, "tp"),
        P("tp", None, None),
        P("tp", None, None),
        P("tp"),
        P("fs"),
        P("tp", "fs"),
        P(),
        P("fs", "tp"),
        P("fs", "tp"),
        P("tp", "fs"),
    )
    body = functools.partial(shards, mesh.shape["fs"], mesh.shape["tp"])
    return jax.shard_map(body, mesh=mesh, in_specs=in_specs, out_specs=P("fs", "tp"), check_vma=False)
```

time: 1100 us -> 435 us (0.40); the launches traced: 1080 us -> 434 us
  local copies, waits for them, and re-layouts: 483 us -> 26.4 us
  waiting for transfers between devices: 477 us -> 257 us
  Pallas kernels: 0 us -> 86 us
  matrix products: 60.6 us -> 0 us
  starting transfers between devices: 0.35 us -> 39.8 us
  other arithmetic: 46.9 us -> 11.1 us
    all_gather x6 -> x0, waiting for transfers between devices: 324 us -> none  [the longest x2 93.4 us: project_down(): lax.all_gather(weight, 'fs', axis=1, tiled=True)]
    slice x15 -> x9, local copies, waits for them, and re-layouts: 330 us -> 7.42 us  [the longest x1 3.6 us: shards(): hidden[chunk * size:(chunk + 1) * size]]
    ppermute x0 -> x38, waiting for transfers between devices: none -> 256 us  [the longest x32 208 us: hop(): return lax.ppermute(value, 'fs', pairs)]
    pad x12 -> x0, local copies, waits for them, and re-layouts: 120 us -> none  [linear_scan(): result = lax.associative_scan(combine_steps, shaped, axis=1)]
    pallas_call x0 -> x5, Pallas kernels: none -> 86 us  [the longest x3 39.1 us: project_down(): pl.pallas_call(functools.partial(down_kernel, groups), grid_spec=pltpu.Pr...]
    reduce_scatter x2 -> x0, waiting for transfers between devices: 85.4 us -> none  [the longest x1 42.7 us: shards(): lax.psum_scatter(down_term.astype(jnp.bfloat16), 'tp', scatter_dimension=...]
    dot_general x7 -> x0, matrix products: 60.6 us -> none  [the longest x2 33.6 us: project_down(): jnp.dot(values, lax.all_gather(weight, 'fs', axis=1, tiled=True), preferr...]
    ppermute x0 -> x38, starting transfers between devices: none -> 39.8 us  [the longest x32 34.4 us: hop(): return lax.ppermute(value, 'fs', pairs)]
  transfers between devices with their start and end apart: 10 -> 40, of which waited for: 8 -> 18; matrix products, arithmetic and copies ran while one was open for 51% -> 6% of each run, Pallas kernels for 0% -> 3%
where the time goes in v1:
time: 435 us; the launch traced here: 434 us
  waiting for transfers between devices  257 us (59%)
  Pallas kernels  86 us (20%)
  starting transfers between devices  39.8 us (9%)
  local copies, waits for them, and re-layouts  26.4 us (6%)
  between operations  13.9 us (3%)
  other arithmetic  11.1 us (3%)
    ppermute x32, waiting for transfers between devices, hop(): return lax.ppermute(value, 'fs', pairs)  208 us
    ppermute x3, waiting for transfers between devices, scatter_sum(): arrived = widen(lax.ppermute(pair, 'tp', perm))  43.4 us
    pallas_call x3, Pallas kernels, project_down(): pl.pallas_call(functools.partial(down_kernel, groups), grid_spec=pltpu.Pr...  39.1 us
    ppermute x32, starting transfers between devices, hop(): return lax.ppermute(value, 'fs', pairs)  34.4 us
    pallas_call x1, Pallas kernels, mixer(): pl.pallas_call(mixer_kernel, grid_spec=pltpu.PrefetchScalarGridSpec(num_s...  25.1 us
    pallas_call x1, Pallas kernels, hidden_units(): pl.pallas_call(hidden_kernel, grid_spec=pltpu.PrefetchScalarGridSpec(num_...  21.8 us
    ppermute x6, local copies, waits for them, and re-layouts, hop(): return lax.ppermute(value, 'fs', pairs)  9.46 us
  transfers between devices with their start and end apart: 40, of which 18 were waited for; matrix products, arithmetic and copies ran while one was open for 6% of the time, Pallas kernels for 3%

profile of v1, /device:TPU:0, one launch (start us, length us, event | category | flops | bytes accessed | tf_op | source)
XLA Modules:
  0.0 434.0 jit_solution(9616305368136266029)
XLA Ops:
  7.3 1.2 copy.21
  8.5 1.2 copy.22
  10.1 3.1 collective-permute-start
  13.2 16.0 %collective-permute-done = bf16[2,256,704]{1,2,0:T(8,128)(2,1)S(1)} collective-permute-done((bf16[2,256,704]{1,2,0:T(8,128)(2,1)S(1)}, bf16[2,256,704]{1,2,0:T(8,128)(2,1)S(1)}, u32[]{:S(2)}, u32[]{:S(2)}) %collective-permute-start) | collective-permute-done | bytes 720928 | tf_op jit(solution)/shard_map/ppermute | solution.py:39
  29.3 1.8 collective-permute-start.2
  31.3 1.8 collective-permute-start.8
  33.3 14.9 %collective-permute-done.2 = bf16[2,256,704]{1,2,0:T(8,128)(2,1)S(1)} collective-permute-done((bf16[2,256,704]{1,2,0:T(8,128)(2,1)S(1)}, bf16[2,256,704]{1,2,0:T(8,128)(2,1)S(1)}, u32[]{:S(2)}, u32[]{:S(2)}) %collective-permute-start.2) | collective-permute-done | bytes 720928 | tf_op jit(solution)/shard_map/ppermute | solution.py:39
  48.3 1.8 collective-permute-start.4
  50.4 5.6 %collective-permute-done.8.rest_1_ = bf16[704,256]{1,0:T(8,128)(2,1)S(1)} collective-permute-done((bf16[704,256]{1,0:T(8,128)(2,1)S(1)}, bf16[704,256]{1,0:T(8,128)(2,1)S(1)}, u32[]{:S(2)}, u32[]{:S(2)}) %collective-permute-start.8) | collective-permute-done | bytes 360480 | tf_op jit(solution)/shard_map/ppermute | solution.py:39
  56.0 1.8 collective-permute-start.10
  58.0 19.6 %collective-permute-done.10.rest_3_ = bf16[704,256]{1,0:T(8,128)(2,1)} collective-permute-done((bf16[704,256]{1,0:T(8,128)(2,1)S(1)}, bf16[704,256]{1,0:T(8,128)(2,1)}, u32[]{:S(2)}, u32[]{:S(2)}) %collective-permute-start.10) | collective-permute-done | bytes 360480 | tf_op jit(solution)/shard_map/ppermute | solution.py:39
  77.7 1.5 collective-permute-start.12
  79.8 3.3 broadcast_multiply_fusion
  83.1 1.4 copy.32.rest_5_
  84.5 1.6 collective-permute-start.6
  86.1 2.3 copy.33.rest_6_
  88.4 1.8 slice.89
  90.7 1.7 mul.45.recur_ref
  92.4 1.7 mul.48.inject_ref
  94.1 1.0 copy.27.token_ref
  95.7 0.9 slice.90
  96.7 1.6 collective-permute-start.14
  98.3 0.9 slice.91
  99.2 0.7 collective-permute-start.15
  101.2 1.2 copy.28.rest_1_
  102.4 1.2 copy.29.rest_2_
  103.6 1.4 collective-permute-done.15
  104.9 0.8 pad_maximum_fusion.2.rest_7_
  105.7 1.2 copy.30.rest_3_
  106.9 2.3 copy.31.rest_4_
  109.2 25.1 %shard_map.145.values_ref = bf16[1024,704]{1,0:T(8,128)(2,1)} custom-call(s32[8]{0:T(128)} %copy-done.24, bf16[1024,2048]{1,0:T(8,128)(2,1)} %all-gather.3.cloned.1.call-done.rows_ref, f32[1,2048]{1,0:T(1,128)} %bitcast.32, f32[4,704]{1,0:T(4,128)} %taps_ref.1, bf16[704,704]{1,0:T(8,128)(2,1)} %mul.45.recur_ref, bf16[704,704]{1,0:T(8,128)(2,1)} %mul.48.inject_ref, ...), custom_call_target="tpu_custom_call" | custom-call | flops 7935623168 | bytes 5767168 | tf_op jit(solution)/shard_map/pallas_call | solution.py:135
  134.3 13.3 %shard_map.146 = (bf16[2,1024,512]{2,1,0:T(8,128)(2,1)}, bf16[2,1024,512]{2,1,0:T(8,128)(2,1)}) custom-call(s32[10]{0:T(128)} %pad_add_fusion.where_ref, bf16[1024,704]{1,0:T(8,128)(2,1)} %shard_map.145.values_ref, bf16[704,256]{1,0:T(8,128)(2,1)} %rest_0_.3, bf16[704,256]{1,0:T(8,128)(2,1)} %copy-done.35, bf16[704,256]{1,0:T(8,128)(2,1)} %copy-done.36, ...), custom_call_target="tpu_custom_call" | custom-call | flops 2952790016 | bytes 2883584 | tf_op jit(solution)/shard_map/pallas_call | solution.py:238
  147.7 4.4 %collective-permute-done.16 = bf16[2,1024,512]{2,1,0:T(8,128)(2,1)S(1)} collective-permute-done((bf16[2,1024,512]{2,1,0:T(8,128)(2,1)}, bf16[2,1024,512]{2,1,0:T(8,128)(2,1)S(1)}, u32[]{:S(2)}, u32[]{:S(2)}) %collective-permute-start.16) | collective-permute-done | bytes 2097184 | tf_op jit(solution)/shard_map/ppermute | solution.py:256
  152.0 1.5 fusion.3
  153.6 1.6 collective-permute-start.17
  155.1 23.7 %collective-permute-done.17 = bf16[1024,512]{1,0:T(8,128)(2,1)S(1)} collective-permute-done((bf16[1024,512]{1,0:T(8,128)(2,1)S(1)}, bf16[1024,512]{1,0:T(8,128)(2,1)S(1)}, u32[]{:S(2)}, u32[]{:S(2)}) %collective-permute-start.17) | collective-permute-done | bytes 1048608 | tf_op jit(solution)/shard_map/ppermute | solution.py:262
  178.8 1.5 fusion.2
  180.6 1.6 collective-permute-start.18
  182.6 30.7 %collective-permute-done.18.rest_1_ = bf16[2,256,1408]{2,1,0:T(8,128)(2,1)S(1)} collective-permute-done((bf16[2,256,1408]{2,1,0:T(8,128)(2,1)S(1)}, bf16[2,256,1408]{2,1,0:T(8,128)(2,1)S(1)}, u32[]{:S(2)}, u32[]{:S(2)}) %collective-permute-start.18) | collective-permute-done | bytes 1441824 | tf_op jit(solution)/shard_map/ppermute | solution.py:39
  213.4 1.6 collective-permute-start.20
  215.4 1.6 collective-permute-start.26
  217.4 30.4 %collective-permute-done.20.rest_3_ = bf16[2,256,1408]{2,1,0:T(8,128)(2,1)S(1)} collective-permute-done((bf16[2,256,1408]{2,1,0:T(8,128)(2,1)S(1)}, bf16[2,256,1408]{2,1,0:T(8,128)(2,1)S(1)}, u32[]{:S(2)}, u32[]{:S(2)}) %collective-permute-start.20) | collective-permute-done | bytes 1441824 | tf_op jit(solution)/shard_map/ppermute | solution.py:39
  247.8 1.6 collective-permute-start.22
  249.9 13.4 %collective-permute-done.26.rest_1_ = bf16[1408,256]{1,0:T(8,128)(2,1)S(1)} collective-permute-done((bf16[1408,256]{1,0:T(8,128)(2,1)}, bf16[1408,256]{1,0:T(8,128)(2,1)S(1)}, u32[]{:S(2)}, u32[]{:S(2)}) %collective-permute-start.26) | collective-permute-done | bytes 720928 | tf_op jit(solution)/shard_map/ppermute | solution.py:39
  263.3 1.6 collective-permute-start.28
  265.3 41.9 %collective-permute-done.28.rest_3_ = bf16[1408,256]{1,0:T(8,128)(2,1)S(1)} collective-permute-done((bf16[1408,256]{1,0:T(8,128)(2,1)S(1)}, bf16[1408,256]{1,0:T(8,128)(2,1)S(1)}, u32[]{:S(2)}, u32[]{:S(2)}) %collective-permute-start.28) | collective-permute-done | bytes 720928 | tf_op jit(solution)/shard_map/ppermute | solution.py:39
  307.2 1.6 collective-permute-start.30
  309.4 1.6 collective-permute-start.24
  311.6 14.6 %collective-permute-done.30.rest_5_ = bf16[1408,256]{1,0:T(8,128)(2,1)S(1)} collective-permute-done((bf16[1408,256]{1,0:T(8,128)(2,1)S(1)}, bf16[1408,256]{1,0:T(8,128)(2,1)S(1)}, u32[]{:S(2)}, u32[]{:S(2)}) %collective-permute-start.30) | collective-permute-done | bytes 720928 | tf_op jit(solution)/shard_map/ppermute | solution.py:39
  326.2 1.6 collective-permute-start.32
  328.6 17.4 %collective-permute-done.32 = bf16[704,256]{1,0:T(8,128)(2,1)S(1)} collective-permute-done((bf16[704,256]{1,0:T(8,128)(2,1)S(1)}, bf16[704,256]{1,0:T(8,128)(2,1)S(1)}, u32[]{:S(2)}, u32[]{:S(2)}) %collective-permute-start.32) | collective-permute-done | bytes 360480 | tf_op jit(solution)/shard_map/ppermute | solution.py:39
  346.1 1.3 collective-permute-done.33
  347.6 0.9 copy-done.33
  348.5 21.8 %shard_map.147 = bf16[1024,1408]{1,0:T(8,128)(2,1)} custom-call(s32[8]{0:T(128)} %copy-done.24, bf16[1024,2048]{1,0:T(8,128)(2,1)} %all-gather.5.cloned.1.call-done.rows_ref, f32[1,2048]{1,0:T(1,128)} %bitcast.33, bf16[2,256,1408]{2,1,0:T(8,128)(2,1)} %copy-done.5, bf16[2,256,1408]{2,1,0:T(8,128)(2,1)} %copy-done.25, bf16[2,256,1408]{2,1,0:T(8,128)(2,1)} %copy-done.26, ...), custom_call_target="tpu_custom_call" | custom-call | flops 11811160064 | bytes 11534336 | tf_op jit(solution)/shard_map/pallas_call | solution.py:188
  370.3 3.6 fusion.7
  373.9 12.9 %shard_map.148 = (bf16[2,512,512]{2,1,0:T(8,128)(2,1)}, bf16[2,512,512]{2,1,0:T(8,128)(2,1)}) custom-call(s32[10]{0:T(128)} %pad_add_fusion.where_ref, bf16[512,1408]{1,0:T(8,128)(2,1)} %get-tuple-element.17.values_ref, bf16[1408,256]{1,0:T(8,128)(2,1)} %rest_0_.5, bf16[1408,256]{1,0:T(8,128)(2,1)} %copy-done.29, bf16[1408,256]{1,0:T(8,128)(2,1)} %copy-done.30, ...), custom_call_target="tpu_custom_call" | custom-call | flops 2952790016 | bytes 5767168 | tf_op jit(solution)/shard_map/pallas_call | solution.py:238
  386.8 13.0 %shard_map.149 = (bf16[2,512,512]{2,1,0:T(8,128)(2,1)}, bf16[2,512,512]{2,1,0:T(8,128)(2,1)}) custom-call(s32[10]{0:T(128)} %pad_add_fusion.where_ref, bf16[512,1408]{1,0:T(8,128)(2,1)} %get-tuple-element.18.values_ref, bf16[1408,256]{1,0:T(8,128)(2,1)} %rest_0_.5, bf16[1408,256]{1,0:T(8,128)(2,1)} %copy-done.29, bf16[1408,256]{1,0:T(8,128)(2,1)} %copy-done.30, ...), custom_call_target="tpu_custom_call" | custom-call | flops 2952790016 | bytes 5767168 | tf_op jit(solution)/shard_map/pallas_call | solution.py:238
  400.4 1.6 collective-permute-start.35
  402.0 0.8 collective-permute-done.36
  402.8 1.3 fusion.5
  404.1 1.6 collective-permute-start.37
  405.7 9.6 %collective-permute-done.35 = bf16[512,512]{1,0:T(8,128)(2,1)S(1)} collective-permute-done((bf16[512,512]{1,0:T(8,128)(2,1)S(1)}, bf16[512,512]{1,0:T(8,128)(2,1)S(1)}, u32[]{:S(2)}, u32[]{:S(2)}) %collective-permute-start.35) | collective-permute-done | bytes 524320 | tf_op jit(solution)/shard_map/ppermute | solution.py:262
  415.5 10.1 %collective-permute-done.37 = bf16[512,512]{1,0:T(8,128)(2,1)S(1)} collective-permute-done((bf16[512,512]{1,0:T(8,128)(2,1)S(1)}, bf16[512,512]{1,0:T(8,128)(2,1)S(1)}, u32[]{:S(2)}, u32[]{:S(2)}) %collective-permute-start.37) | collective-permute-done | bytes 524320 | tf_op jit(solution)/shard_map/ppermute | solution.py:262
  425.8 1.3 fusion
  (136 shorter events, 10.5 us)
Async XLA Ops:
  6.5 102.7 %all-gather.3.cloned.1.call-start = ((), (), s32[]{:S(2)}) async-start(), calls=%async_computation | async-start | bytes 5242880 | tf_op jit(solution)/shard_map/all_gather | solution.py:296
  7.3 341.3 %all-gather.5.cloned.1.call-start = ((), (), s32[]{:S(2)}) async-start(), calls=%async_computation.1 | async-start | bytes 5242880 | tf_op jit(solution)/shard_map/all_gather | solution.py:311
  8.5 22.8 %copy-start.34 = (bf16[704,256]{1,0:T(8,128)(2,1)S(1)}, bf16[704,256]{1,0:T(8,128)(2,1)}, u32[]{:S(2)}) copy-start(bf16[704,256]{1,0:T(8,128)(2,1)} %rest_0_.3) | copy-start | bytes 1081348
  8.5 71.3 %copy-start.16 = (bf16[2,352,352]{2,1,0:T(8,128)(2,1)S(1)}, bf16[2,352,352]{2,1,0:T(8,128)(2,1)}, u32[]{:S(2)}) copy-start(bf16[2,352,352]{2,1,0:T(8,128)(2,1)} %param.21) | copy-start | bytes 1486852
  9.8 73.2 %copy-start.2 = (bf16[2,256,704]{2,1,0:T(8,128)(2,1)}, bf16[2,256,704]{2,1,0:T(8,128)(2,1)S(1)}, u32[]{:S(2)}) copy-start(bf16[2,256,704]{2,1,0:T(8,128)(2,1)S(1)} %pad_maximum_fusion.1.rest_0_) | copy-start | bytes 2162692
  10.1 19.2 %collective-permute-start = (bf16[2,256,704]{1,2,0:T(8,128)(2,1)S(1)}, bf16[2,256,704]{1,2,0:T(8,128)(2,1)S(1)}, u32[]{:S(2)}, u32[]{:S(2)}) collective-permute-start(bf16[2,256,704]{1,2,0:T(8,128)(2,1)S(1)} %copy.23), channel_id=1, source_target_pairs={{0,8},{8,16},{16,24},{24,28},{28,20},{20,12},{12,4},{4,0},{1,9},{9... | collective-permute-start | bytes 2162696 | tf_op jit(solution)/shard_map/ppermute | solution.py:39
  13.2 17.9 %collective-permute-start.1 = (bf16[2,256,704]{1,2,0:T(8,128)(2,1)S(1)}, bf16[2,256,704]{1,2,0:T(8,128)(2,1)S(1)}, u32[]{:S(2)}, u32[]{:S(2)}) collective-permute-start(bf16[2,256,704]{1,2,0:T(8,128)(2,1)S(1)} %copy.23), channel_id=1, source_target_pairs={{0,4},{8,0},{16,8},{24,16},{28,24},{20,28},{12,20},{4,12},{1,5},{9... | collective-permute-start | bytes 2162696 | tf_op jit(solution)/shard_map/ppermute | solution.py:39
  29.3 19.0 %collective-permute-start.2 = (bf16[2,256,704]{1,2,0:T(8,128)(2,1)S(1)}, bf16[2,256,704]{1,2,0:T(8,128)(2,1)S(1)}, u32[]{:S(2)}, u32[]{:S(2)}) collective-permute-start(bf16[2,256,704]{1,2,0:T(8,128)(2,1)S(1)} %collective-permute-done), channel_id=1, source_target_pairs={{0,8},{8,16},{16,24},{24,28},{28,20},{20,12},{12,4},{4,0},{1,9},{9... | collective-permute-start | bytes 2162696 | tf_op jit(solution)/shard_map/ppermute | solution.py:39
  31.1 19.1 %collective-permute-start.3 = (bf16[2,256,704]{1,2,0:T(8,128)(2,1)S(1)}, bf16[2,256,704]{1,2,0:T(8,128)(2,1)}, u32[]{:S(2)}, u32[]{:S(2)}) collective-permute-start(bf16[2,256,704]{1,2,0:T(8,128)(2,1)S(1)} %collective-permute-done.1), channel_id=1, source_target_pairs={{0,4},{8,0},{16,8},{24,16},{28,24},{20,28},{12,20},{4,12},{1,5},{9... | collective-permute-start | bytes 2162696 | tf_op jit(solution)/shard_map/ppermute | solution.py:39
  31.3 24.7 %collective-permute-start.8 = (bf16[704,256]{1,0:T(8,128)(2,1)S(1)}, bf16[704,256]{1,0:T(8,128)(2,1)S(1)}, u32[]{:S(2)}, u32[]{:S(2)}) collective-permute-start(bf16[704,256]{1,0:T(8,128)(2,1)S(1)} %copy-done.34), channel_id=1, source_target_pairs={{0,8},{8,16},{16,24},{24,28},{28,20},{20,12},{12,4},{4,0},{1,9},{9... | collective-permute-start | bytes 1081352 | tf_op jit(solution)/shard_map/ppermute | solution.py:39
  33.1 24.7 %collective-permute-start.9 = (bf16[704,256]{1,0:T(8,128)(2,1)S(1)}, bf16[704,256]{1,0:T(8,128)(2,1)S(1)}, u32[]{:S(2)}, u32[]{:S(2)}) collective-permute-start(bf16[704,256]{1,0:T(8,128)(2,1)S(1)} %copy-done.34), channel_id=1, source_target_pairs={{0,4},{8,0},{16,8},{24,16},{28,24},{20,28},{12,20},{4,12},{1,5},{9... | collective-permute-start | bytes 1081352 | tf_op jit(solution)/shard_map/ppermute | solution.py:39
  48.3 34.8 %copy-start.8 = (bf16[2,256,704]{1,2,0:T(8,128)(2,1)}, bf16[2,256,704]{1,2,0:T(8,128)(2,1)S(1)}, u32[]{:S(2)}) copy-start(bf16[2,256,704]{1,2,0:T(8,128)(2,1)S(1)} %collective-permute-done.2) | copy-start | bytes 2162692
  48.3 34.8 %collective-permute-start.4 = (bf16[2,256,704]{1,2,0:T(8,128)(2,1)S(1)}, bf16[2,256,704]{1,2,0:T(8,128)(2,1)}, u32[]{:S(2)}, u32[]{:S(2)}) collective-permute-start(bf16[2,256,704]{1,2,0:T(8,128)(2,1)S(1)} %collective-permute-done.2), channel_id=1, source_target_pairs={{0,8},{8,16},{16,24},{24,28},{28,20},{20,12},{12,4},{4,0},{1,9},{9... | collective-permute-start | bytes 2162696 | tf_op jit(solution)/shard_map/ppermute | solution.py:39
  50.2 35.9 %collective-permute-start.5 = (bf16[2,256,704]{1,2,0:T(8,128)(2,1)}, bf16[2,256,704]{1,2,0:T(8,128)(2,1)}, u32[]{:S(2)}, u32[]{:S(2)}) collective-permute-start(bf16[2,256,704]{1,2,0:T(8,128)(2,1)} %collective-permute-done.3), channel_id=1, source_target_pairs={{0,4},{8,0},{16,8},{24,16},{28,24},{20,28},{12,20},{4,12},{1,5},{9... | collective-permute-start | bytes 2162696 | tf_op jit(solution)/shard_map/ppermute | solution.py:39
  56.0 23.2 %copy-start.35 = (bf16[704,256]{1,0:T(8,128)(2,1)}, bf16[704,256]{1,0:T(8,128)(2,1)S(1)}, u32[]{:S(2)}) copy-start(bf16[704,256]{1,0:T(8,128)(2,1)S(1)} %collective-permute-done.8.rest_1_) | copy-start | bytes 1081348
  56.0 21.7 %collective-permute-start.10 = (bf16[704,256]{1,0:T(8,128)(2,1)S(1)}, bf16[704,256]{1,0:T(8,128)(2,1)}, u32[]{:S(2)}, u32[]{:S(2)}) collective-permute-start(bf16[704,256]{1,0:T(8,128)(2,1)S(1)} %collective-permute-done.8.rest_1_), channel_id=1, source_target_pairs={{0,8},{8,16},{16,24},{24,28},{28,20},{20,12},{12,4},{4,0},{1,9},{9... | collective-permute-start | bytes 1081352 | tf_op jit(solution)/shard_map/ppermute | solution.py:39
  57.8 21.4 %copy-start.36 = (bf16[704,256]{1,0:T(8,128)(2,1)}, bf16[704,256]{1,0:T(8,128)(2,1)S(1)}, u32[]{:S(2)}) copy-start(bf16[704,256]{1,0:T(8,128)(2,1)S(1)} %collective-permute-done.9.rest_2_) | copy-start | bytes 1081348
  57.8 21.4 %collective-permute-start.11 = (bf16[704,256]{1,0:T(8,128)(2,1)S(1)}, bf16[704,256]{1,0:T(8,128)(2,1)}, u32[]{:S(2)}, u32[]{:S(2)}) collective-permute-start(bf16[704,256]{1,0:T(8,128)(2,1)S(1)} %collective-permute-done.9.rest_2_), channel_id=1, source_target_pairs={{0,4},{8,0},{16,8},{24,16},{28,24},{20,28},{12,20},{4,12},{1,5},{9... | collective-permute-start | bytes 1081352 | tf_op jit(solution)/shard_map/ppermute | solution.py:39
  77.7 18.1 %collective-permute-start.12 = (bf16[704,256]{1,0:T(8,128)(2,1)}, bf16[704,256]{1,0:T(8,128)(2,1)}, u32[]{:S(2)}, u32[]{:S(2)}) collective-permute-start(bf16[704,256]{1,0:T(8,128)(2,1)} %collective-permute-done.10.rest_3_), channel_id=1, source_target_pairs={{0,8},{8,16},{16,24},{24,28},{28,20},{20,12},{12,4},{4,0},{1,9},{9... | collective-permute-start | bytes 1081352 | tf_op jit(solution)/shard_map/ppermute | solution.py:39
  79.2 19.0 %collective-permute-start.13 = (bf16[704,256]{1,0:T(8,128)(2,1)}, bf16[704,256]{1,0:T(8,128)(2,1)}, u32[]{:S(2)}, u32[]{:S(2)}) collective-permute-start(bf16[704,256]{1,0:T(8,128)(2,1)} %collective-permute-done.11.rest_4_), channel_id=1, source_target_pairs={{0,4},{8,0},{16,8},{24,16},{28,24},{20,28},{12,20},{4,12},{1,5},{9... | collective-permute-start | bytes 1081352 | tf_op jit(solution)/shard_map/ppermute | solution.py:39
  84.5 24.7 %collective-permute-start.6 = (bf16[1,256,704]{2,1,0:T(8,128)(2,1)S(1)}, bf16[1,256,704]{2,1,0:T(8,128)(2,1)}, u32[]{:S(2)}, u32[]{:S(2)}) collective-permute-start(bf16[1,256,704]{2,1,0:T(8,128)(2,1)S(1)} %slice.88), channel_id=1, source_target_pairs={{0,8},{8,16},{16,24},{24,28},{28,20},{20,12},{12,4},{4,0},{1,9},{9... | collective-permute-start | bytes 1081352 | tf_op jit(solution)/shard_map/ppermute | solution.py:39
  90.2 19.0 %collective-permute-start.7 = (bf16[1,256,704]{2,1,0:T(8,128)(2,1)}, bf16[1,256,704]{2,1,0:T(8,128)(2,1)}, u32[]{:S(2)}, u32[]{:S(2)}) collective-permute-start(bf16[1,256,704]{2,1,0:T(8,128)(2,1)} %slice.89), channel_id=1, source_target_pairs={{0,4},{8,0},{16,8},{24,16},{28,24},{20,28},{12,20},{4,12},{1,5},{9... | collective-permute-start | bytes 1081352 | tf_op jit(solution)/shard_map/ppermute | solution.py:39
  96.7 6.9 %collective-permute-start.14 = (bf16[352,256]{1,0:T(8,128)(2,1)S(1)}, bf16[352,256]{1,0:T(8,128)(2,1)S(1)}, u32[]{:S(2)}, u32[]{:S(2)}) collective-permute-start(bf16[352,256]{1,0:T(8,128)(2,1)S(1)} %slice.90), channel_id=1, source_target_pairs={{0,8},{8,16},{16,24},{24,28},{28,20},{20,12},{12,4},{4,0},{1,9},{9... | collective-permute-start | bytes 540680 | tf_op jit(solution)/shard_map/ppermute | solution.py:39
  99.2 5.7 %collective-permute-start.15 = (bf16[352,256]{1,0:T(8,128)(2,1)S(1)}, bf16[352,256]{1,0:T(8,128)(2,1)S(1)}, u32[]{:S(2)}, u32[]{:S(2)}) collective-permute-start(bf16[352,256]{1,0:T(8,128)(2,1)S(1)} %slice.91), channel_id=1, source_target_pairs={{0,4},{8,0},{16,8},{24,16},{28,24},{20,28},{12,20},{4,12},{1,5},{9... | collective-permute-start | bytes 540680 | tf_op jit(solution)/shard_map/ppermute | solution.py:39
  147.6 31.2 %copy-start.1 = (bf16[1024,512]{1,0:T(8,128)(2,1)S(1)}, bf16[1024,512]{1,0:T(8,128)(2,1)}, u32[]{:S(2)}) copy-start(bf16[1024,512]{1,0:T(8,128)(2,1)} %param.15) | copy-start | bytes 3145732
  147.6 31.2 %copy-start.3 = (bf16[2,1024,512]{2,1,0:T(8,128)(2,1)S(1)}, bf16[2,1024,512]{2,1,0:T(8,128)(2,1)}, u32[]{:S(2)}) copy-start(bf16[2,1024,512]{2,1,0:T(8,128)(2,1)} %get-tuple-element.11) | copy-start | bytes 6291460
  147.6 4.4 %collective-permute-start.16 = (bf16[2,1024,512]{2,1,0:T(8,128)(2,1)}, bf16[2,1024,512]{2,1,0:T(8,128)(2,1)S(1)}, u32[]{:S(2)}, u32[]{:S(2)}) collective-permute-start(bf16[2,1024,512]{2,1,0:T(8,128)(2,1)} %get-tuple-element.12), channel_id=1, source_target_pairs={{0,1},{1,0},{2,3},{3,2},{4,5},{5,4},{6,7},{7,6},{8,9},{9,8},{10,11... | collective-permute-start | bytes 6291464 | tf_op jit(solution)/shard_map/ppermute | solution.py:256
  153.5 26.8 %copy-start.14 = (bf16[256,1408]{1,0:T(8,128)(2,1)S(1)}, bf16[256,1408]{1,0:T(8,128)(2,1)}, u32[]{:S(2)}) copy-start(bf16[256,1408]{1,0:T(8,128)(2,1)} %param.27) | copy-start | bytes 2162692
  153.5 26.8 %copy-start.15 = (bf16[256,1408]{1,0:T(8,128)(2,1)S(1)}, bf16[256,1408]{1,0:T(8,128)(2,1)}, u32[]{:S(2)}) copy-start(bf16[256,1408]{1,0:T(8,128)(2,1)} %param.26) | copy-start | bytes 2162692
  153.6 25.3 %collective-permute-start.17 = (bf16[1024,512]{1,0:T(8,128)(2,1)S(1)}, bf16[1024,512]{1,0:T(8,128)(2,1)S(1)}, u32[]{:S(2)}, u32[]{:S(2)}) collective-permute-start(bf16[1024,512]{1,0:T(8,128)(2,1)S(1)} %fusion.3), channel_id=1, source_target_pairs={{0,2},{1,3},{2,0},{3,1},{4,6},{5,7},{6,4},{7,5},{8,10},{9,11},{10,... | collective-permute-start | bytes 3145736 | tf_op jit(solution)/shard_map/ppermute | solution.py:262
  180.5 147.4 %copy-start.5 = (bf16[2,256,1408]{2,1,0:T(8,128)(2,1)}, bf16[2,256,1408]{2,1,0:T(8,128)(2,1)S(1)}, u32[]{:S(2)}) copy-start(bf16[2,256,1408]{2,1,0:T(8,128)(2,1)S(1)} %pad_maximum_fusion.rest_0_) | copy-start | bytes 4325380
  180.6 32.8 %collective-permute-start.18 = (bf16[2,256,1408]{2,1,0:T(8,128)(2,1)S(1)}, bf16[2,256,1408]{2,1,0:T(8,128)(2,1)S(1)}, u32[]{:S(2)}, u32[]{:S(2)}) collective-permute-start(bf16[2,256,1408]{2,1,0:T(8,128)(2,1)S(1)} %pad_maximum_fusion.rest_0_), channel_id=1, source_target_pairs={{0,8},{8,16},{16,24},{24,28},{28,20},{20,12},{12,4},{4,0},{1,9},{9... | collective-permute-start | bytes 4325384 | tf_op jit(solution)/shard_map/ppermute | solution.py:39
  182.2 32.8 %collective-permute-start.19 = (bf16[2,256,1408]{2,1,0:T(8,128)(2,1)S(1)}, bf16[2,256,1408]{2,1,0:T(8,128)(2,1)S(1)}, u32[]{:S(2)}, u32[]{:S(2)}) collective-permute-start(bf16[2,256,1408]{2,1,0:T(8,128)(2,1)S(1)} %pad_maximum_fusion.rest_0_), channel_id=1, source_target_pairs={{0,4},{8,0},{16,8},{24,16},{28,24},{20,28},{12,20},{4,12},{1,5},{9... | collective-permute-start | bytes 4325384 | tf_op jit(solution)/shard_map/ppermute | solution.py:39
  213.4 95.9 %copy-start.25 = (bf16[2,256,1408]{2,1,0:T(8,128)(2,1)}, bf16[2,256,1408]{2,1,0:T(8,128)(2,1)S(1)}, u32[]{:S(2)}) copy-start(bf16[2,256,1408]{2,1,0:T(8,128)(2,1)S(1)} %collective-permute-done.18.rest_1_) | copy-start | bytes 4325380
  213.4 34.5 %collective-permute-start.20 = (bf16[2,256,1408]{2,1,0:T(8,128)(2,1)S(1)}, bf16[2,256,1408]{2,1,0:T(8,128)(2,1)S(1)}, u32[]{:S(2)}, u32[]{:S(2)}) collective-permute-start(bf16[2,256,1408]{2,1,0:T(8,128)(2,1)S(1)} %collective-permute-done.18.rest_1_), channel_id=1, source_target_pairs={{0,8},{8,16},{16,24},{24,28},{28,20},{20,12},{12,4},{4,0},{1,9},{9... | collective-permute-start | bytes 4325384 | tf_op jit(solution)/shard_map/ppermute | solution.py:39
  215.0 94.3 %copy-start.26 = (bf16[2,256,1408]{2,1,0:T(8,128)(2,1)}, bf16[2,256,1408]{2,1,0:T(8,128)(2,1)S(1)}, u32[]{:S(2)}) copy-start(bf16[2,256,1408]{2,1,0:T(8,128)(2,1)S(1)} %collective-permute-done.19.rest_2_) | copy-start | bytes 4325380
  215.0 34.5 %collective-permute-start.21 = (bf16[2,256,1408]{2,1,0:T(8,128)(2,1)S(1)}, bf16[2,256,1408]{2,1,0:T(8,128)(2,1)S(1)}, u32[]{:S(2)}, u32[]{:S(2)}) collective-permute-start(bf16[2,256,1408]{2,1,0:T(8,128)(2,1)S(1)} %collective-permute-done.19.rest_2_), channel_id=1, source_target_pairs={{0,4},{8,0},{16,8},{24,16},{28,24},{20,28},{12,20},{4,12},{1,5},{9... | collective-permute-start | bytes 4325384 | tf_op jit(solution)/shard_map/ppermute | solution.py:39
  215.4 47.9 %collective-permute-start.26 = (bf16[1408,256]{1,0:T(8,128)(2,1)}, bf16[1408,256]{1,0:T(8,128)(2,1)S(1)}, u32[]{:S(2)}, u32[]{:S(2)}) collective-permute-start(bf16[1408,256]{1,0:T(8,128)(2,1)} %rest_0_.5), channel_id=1, source_target_pairs={{0,8},{8,16},{16,24},{24,28},{28,20},{20,12},{12,4},{4,0},{1,9},{9... | collective-permute-start | bytes 2162696 | tf_op jit(solution)/shard_map/ppermute | solution.py:39
  217.0 47.9 %collective-permute-start.27 = (bf16[1408,256]{1,0:T(8,128)(2,1)}, bf16[1408,256]{1,0:T(8,128)(2,1)S(1)}, u32[]{:S(2)}, u32[]{:S(2)}) collective-permute-start(bf16[1408,256]{1,0:T(8,128)(2,1)} %rest_0_.5), channel_id=1, source_target_pairs={{0,4},{8,0},{16,8},{24,16},{28,24},{20,28},{12,20},{4,12},{1,5},{9... | collective-permute-start | bytes 2162696 | tf_op jit(solution)/shard_map/ppermute | solution.py:39
  247.8 99.7 %copy-start.27 = (bf16[2,256,1408]{2,1,0:T(8,128)(2,1)}, bf16[2,256,1408]{2,1,0:T(8,128)(2,1)S(1)}, u32[]{:S(2)}) copy-start(bf16[2,256,1408]{2,1,0:T(8,128)(2,1)S(1)} %collective-permute-done.20.rest_3_) | copy-start | bytes 4325380
  247.8 61.5 %collective-permute-start.22 = (bf16[2,256,1408]{2,1,0:T(8,128)(2,1)S(1)}, bf16[2,256,1408]{2,1,0:T(8,128)(2,1)S(1)}, u32[]{:S(2)}, u32[]{:S(2)}) collective-permute-start(bf16[2,256,1408]{2,1,0:T(8,128)(2,1)S(1)} %collective-permute-done.20.rest_3_), channel_id=1, source_target_pairs={{0,8},{8,16},{16,24},{24,28},{28,20},{20,12},{12,4},{4,0},{1,9},{9... | collective-permute-start | bytes 4325384 | tf_op jit(solution)/shard_map/ppermute | solution.py:39
  249.4 98.1 %copy-start.28 = (bf16[2,256,1408]{2,1,0:T(8,128)(2,1)}, bf16[2,256,1408]{2,1,0:T(8,128)(2,1)S(1)}, u32[]{:S(2)}) copy-start(bf16[2,256,1408]{2,1,0:T(8,128)(2,1)S(1)} %collective-permute-done.21.rest_4_) | copy-start | bytes 4325380
  249.4 61.6 %collective-permute-start.23 = (bf16[2,256,1408]{2,1,0:T(8,128)(2,1)S(1)}, bf16[2,256,1408]{2,1,0:T(8,128)(2,1)S(1)}, u32[]{:S(2)}, u32[]{:S(2)}) collective-permute-start(bf16[2,256,1408]{2,1,0:T(8,128)(2,1)S(1)} %collective-permute-done.21.rest_4_), channel_id=1, source_target_pairs={{0,4},{8,0},{16,8},{24,16},{28,24},{20,28},{12,20},{4,12},{1,5},{9... | collective-permute-start | bytes 4325384 | tf_op jit(solution)/shard_map/ppermute | solution.py:39
  263.3 46.0 %copy-start.29 = (bf16[1408,256]{1,0:T(8,128)(2,1)}, bf16[1408,256]{1,0:T(8,128)(2,1)S(1)}, u32[]{:S(2)}) copy-start(bf16[1408,256]{1,0:T(8,128)(2,1)S(1)} %collective-permute-done.26.rest_1_) | copy-start | bytes 2162692
  263.3 43.9 %collective-permute-start.28 = (bf16[1408,256]{1,0:T(8,128)(2,1)S(1)}, bf16[1408,256]{1,0:T(8,128)(2,1)S(1)}, u32[]{:S(2)}, u32[]{:S(2)}) collective-permute-start(bf16[1408,256]{1,0:T(8,128)(2,1)S(1)} %collective-permute-done.26.rest_1_), channel_id=1, source_target_pairs={{0,8},{8,16},{16,24},{24,28},{28,20},{20,12},{12,4},{4,0},{1,9},{9... | collective-permute-start | bytes 2162696 | tf_op jit(solution)/shard_map/ppermute | solution.py:39
  264.9 43.9 %copy-start.30 = (bf16[1408,256]{1,0:T(8,128)(2,1)}, bf16[1408,256]{1,0:T(8,128)(2,1)S(1)}, u32[]{:S(2)}) copy-start(bf16[1408,256]{1,0:T(8,128)(2,1)S(1)} %collective-permute-done.27.rest_2_) | copy-start | bytes 2162692
  264.9 43.9 %collective-permute-start.29 = (bf16[1408,256]{1,0:T(8,128)(2,1)S(1)}, bf16[1408,256]{1,0:T(8,128)(2,1)S(1)}, u32[]{:S(2)}, u32[]{:S(2)}) collective-permute-start(bf16[1408,256]{1,0:T(8,128)(2,1)S(1)} %collective-permute-done.27.rest_2_), channel_id=1, source_target_pairs={{0,4},{8,0},{16,8},{24,16},{28,24},{20,28},{12,20},{4,12},{1,5},{9... | collective-permute-start | bytes 2162696 | tf_op jit(solution)/shard_map/ppermute | solution.py:39
  307.2 40.3 %copy-start.31 = (bf16[1408,256]{1,0:T(8,128)(2,1)}, bf16[1408,256]{1,0:T(8,128)(2,1)S(1)}, u32[]{:S(2)}) copy-start(bf16[1408,256]{1,0:T(8,128)(2,1)S(1)} %collective-permute-done.28.rest_3_) | copy-start | bytes 2162692
  307.2 19.0 %collective-permute-start.30 = (bf16[1408,256]{1,0:T(8,128)(2,1)S(1)}, bf16[1408,256]{1,0:T(8,128)(2,1)S(1)}, u32[]{:S(2)}, u32[]{:S(2)}) collective-permute-start(bf16[1408,256]{1,0:T(8,128)(2,1)S(1)} %collective-permute-done.28.rest_3_), channel_id=1, source_target_pairs={{0,8},{8,16},{16,24},{24,28},{28,20},{20,12},{12,4},{4,0},{1,9},{9... | collective-permute-start | bytes 2162696 | tf_op jit(solution)/shard_map/ppermute | solution.py:39
  308.8 38.8 %copy-start.32 = (bf16[1408,256]{1,0:T(8,128)(2,1)}, bf16[1408,256]{1,0:T(8,128)(2,1)S(1)}, u32[]{:S(2)}) copy-start(bf16[1408,256]{1,0:T(8,128)(2,1)S(1)} %collective-permute-done.29.rest_4_) | copy-start | bytes 2162692
  308.8 19.1 %collective-permute-start.31 = (bf16[1408,256]{1,0:T(8,128)(2,1)S(1)}, bf16[1408,256]{1,0:T(8,128)(2,1)S(1)}, u32[]{:S(2)}, u32[]{:S(2)}) collective-permute-start(bf16[1408,256]{1,0:T(8,128)(2,1)S(1)} %collective-permute-done.29.rest_4_), channel_id=1, source_target_pairs={{0,4},{8,0},{16,8},{24,16},{28,24},{20,28},{12,20},{4,12},{1,5},{9... | collective-permute-start | bytes 2162696 | tf_op jit(solution)/shard_map/ppermute | solution.py:39
  309.4 38.1 %collective-permute-start.24 = (bf16[1,256,1408]{2,1,0:T(8,128)(2,1)S(1)}, bf16[1,256,1408]{2,1,0:T(8,128)(2,1)S(1)}, u32[]{:S(2)}, u32[]{:S(2)}) collective-permute-start(bf16[1,256,1408]{2,1,0:T(8,128)(2,1)S(1)} %slice.94), channel_id=1, source_target_pairs={{0,8},{8,16},{16,24},{24,28},{28,20},{20,12},{12,4},{4,0},{1,9},{9... | collective-permute-start | bytes 2162696 | tf_op jit(solution)/shard_map/ppermute | solution.py:39
  311.0 36.5 %copy-start.18 = (bf16[2,256,1408]{2,1,0:T(8,128)(2,1)}, bf16[2,256,1408]{2,1,0:T(8,128)(2,1)S(1)}, u32[]{:S(2)}) copy-start(bf16[2,256,1408]{2,1,0:T(8,128)(2,1)S(1)} %collective-permute-done.23.rest_6_) | copy-start | bytes 4325380
  311.1 37.5 %collective-permute-start.25 = (bf16[1,256,1408]{2,1,0:T(8,128)(2,1)S(1)}, bf16[1,256,1408]{2,1,0:T(8,128)(2,1)}, u32[]{:S(2)}, u32[]{:S(2)}) collective-permute-start(bf16[1,256,1408]{2,1,0:T(8,128)(2,1)S(1)} %slice.95), channel_id=1, source_target_pairs={{0,4},{8,0},{16,8},{24,16},{28,24},{20,28},{12,20},{4,12},{1,5},{9... | collective-permute-start | bytes 2162696 | tf_op jit(solution)/shard_map/ppermute | solution.py:39
  326.2 21.3 %copy-start.19 = (bf16[1408,256]{1,0:T(8,128)(2,1)}, bf16[1408,256]{1,0:T(8,128)(2,1)S(1)}, u32[]{:S(2)}) copy-start(bf16[1408,256]{1,0:T(8,128)(2,1)S(1)} %collective-permute-done.30.rest_5_) | copy-start | bytes 2162692
  326.2 19.9 %collective-permute-start.32 = (bf16[704,256]{1,0:T(8,128)(2,1)S(1)}, bf16[704,256]{1,0:T(8,128)(2,1)S(1)}, u32[]{:S(2)}, u32[]{:S(2)}) collective-permute-start(bf16[704,256]{1,0:T(8,128)(2,1)S(1)} %slice.97), channel_id=1, source_target_pairs={{0,8},{8,16},{16,24},{24,28},{28,20},{20,12},{12,4},{4,0},{1,9},{9... | collective-permute-start | bytes 1081352 | tf_op jit(solution)/shard_map/ppermute | solution.py:39
  327.9 19.5 %collective-permute-start.33 = (bf16[704,256]{1,0:T(8,128)(2,1)S(1)}, bf16[704,256]{1,0:T(8,128)(2,1)S(1)}, u32[]{:S(2)}, u32[]{:S(2)}) collective-permute-start(bf16[704,256]{1,0:T(8,128)(2,1)S(1)} %slice.98), channel_id=1, source_target_pairs={{0,4},{8,0},{16,8},{24,16},{28,24},{20,28},{12,20},{4,12},{1,5},{9... | collective-permute-start | bytes 1081352 | tf_op jit(solution)/shard_map/ppermute | solution.py:39
  347.5 22.8 %copy-start.21 = (bf16[1408,256]{1,0:T(8,128)(2,1)}, bf16[1408,256]{1,0:T(8,128)(2,1)S(1)}, u32[]{:S(2)}) copy-start(bf16[1408,256]{1,0:T(8,128)(2,1)S(1)} %constant_dynamic-update-slice_fusion.rest_7_) | copy-start | bytes 2162692
  386.8 13.5 %collective-permute-start.34 = (bf16[2,512,512]{2,1,0:T(8,128)(2,1)}, bf16[2,512,512]{2,1,0:T(8,128)(2,1)S(1)}, u32[]{:S(2)}, u32[]{:S(2)}) collective-permute-start(bf16[2,512,512]{2,1,0:T(8,128)(2,1)} %get-tuple-element.14), channel_id=1, source_target_pairs={{0,1},{1,0},{2,3},{3,2},{4,5},{5,4},{6,7},{7,6},{8,9},{9,8},{10,11... | collective-permute-start | bytes 3145736 | tf_op jit(solution)/shard_map/ppermute | solution.py:256
  399.8 3.0 collective-permute-start.36
  400.4 14.9 %collective-permute-start.35 = (bf16[512,512]{1,0:T(8,128)(2,1)S(1)}, bf16[512,512]{1,0:T(8,128)(2,1)S(1)}, u32[]{:S(2)}, u32[]{:S(2)}) collective-permute-start(bf16[512,512]{1,0:T(8,128)(2,1)S(1)} %fusion.4), channel_id=1, source_target_pairs={{0,2},{1,3},{2,0},{3,1},{4,6},{5,7},{6,4},{7,5},{8,10},{9,11},{10,... | collective-permute-start | bytes 1572872 | tf_op jit(solution)/shard_map/ppermute | solution.py:262
  402.8 22.8 %copy-start.7 = (bf16[2,512,512]{2,1,0:T(8,128)(2,1)S(1)}, bf16[2,512,512]{2,1,0:T(8,128)(2,1)}, u32[]{:S(2)}) copy-start(bf16[2,512,512]{2,1,0:T(8,128)(2,1)} %get-tuple-element.15) | copy-start | bytes 3145732
  404.1 21.7 %copy-start = (bf16[1024,512]{1,0:T(8,128)(2,1)S(1)}, bf16[1024,512]{1,0:T(8,128)(2,1)}, u32[]{:S(2)}) copy-start(bf16[1024,512]{1,0:T(8,128)(2,1)} %fusion.2) | copy-start | bytes 3145732
  404.1 21.5 %collective-permute-start.37 = (bf16[512,512]{1,0:T(8,128)(2,1)S(1)}, bf16[512,512]{1,0:T(8,128)(2,1)S(1)}, u32[]{:S(2)}, u32[]{:S(2)}) collective-permute-start(bf16[512,512]{1,0:T(8,128)(2,1)S(1)} %fusion.5), channel_id=1, source_target_pairs={{0,2},{1,3},{2,0},{3,1},{4,6},{5,7},{6,4},{7,5},{8,10},{9,11},{10,... | collective-permute-start | bytes 1572872 | tf_op jit(solution)/shard_map/ppermute | solution.py:262
  (13 other events, 143.9 us)
Sparse Core Ops, SparseCore 0:
  8.9 37.1 all-gather.2
  180.5 34.7 all-gather.4
